TPU v7x, 32 devices: a whole 2x2x4 slice. The times are simulated.
32 devices in a mesh: fs: 8 (over z, x), tp: 4 (over y, core).
Axes of the slice: x: 2, y: 2, z: 4, core: 2. Of those that a mesh axis runs over, the one named last changes fastest.
Arguments:
- inputs: bfloat16 [2048, 2048], P('fs'), may hold values from -6 to 6
- cotangent: bfloat16 [2048, 2048], P('fs'), may hold values from -8 to 8
- up_weight: float32 [2048, 2944], P('fs', 'tp'), may hold values from -0.125 to 0.125
- gate_weight: float32 [2048, 2944], P('fs', 'tp'), may hold values from -0.125 to 0.125
- down_weight: float32 [2944, 2048], P('tp', 'fs'), may hold values from -0.109375 to 0.109375
- up_scale: float32 [2944], P('tp'), may hold values from 0.5 to 2
- gate_scale: float32 [2944], P('tp'), may hold values from 0.5 to 2
- down_scale: float32 [2048], replicated, may hold values from 0.5 to 2
- conv_weight: float32 [3, 2944], P(None, 'tp'), may hold values from -3.5 to 3.5
- conv_bias: float32 [2944], P('tp'), may hold values from -3 to 3
Outputs:
- grad_input: bfloat16 [2048, 2048], P('fs')
- grad_up: float32 [2048, 2944], P('fs', 'tp')
- grad_gate: float32 [2048, 2944], P('fs', 'tp')
- grad_down: float32 [2944, 2048], P('tp', 'fs')
- grad_conv: float32 [3, 2944], P(None, 'tp')
- grad_bias: float32 [2944], P('tp')
All inputs are finite; a program needn't handle non-finite values.
Results may differ from a plain program's by a relative error of at most 0.018.
Values may be sent and summed in bfloat16 or wider, within the bound.
A program may use at most 64 MiB of HBM per device.

v0:
```python
import functools

import jax
import jax.numpy as jnp
from jax import lax
from jax.experimental import pallas as pl
from jax.experimental.pallas import tpu as pltpu
from jax.sharding import PartitionSpec as P

TAPS = 3
QUADS = 4
MESH = pl.DeviceIdType.MESH


def causal_conv(act, conv_weight, conv_bias):
    length = act.shape[1]
    padded = jnp.pad(act, ((0, 0), (TAPS - 1, 0), (0, 0)))
    result = conv_bias + jnp.zeros_like(act)
    for offset in range(TAPS):
        result = result + padded[:, offset : offset + length] * conv_weight[offset]
    return (result, padded)


def conv_back(conv_cot, padded, conv_weight):
    length = conv_cot.shape[1]
    padded_cot = jnp.pad(conv_cot, ((0, 0), (0, TAPS - 1), (0, 0)))
    act_cot = jnp.zeros_like(conv_cot)
    tap_grads = []
    for offset in range(TAPS):
        shift_start = TAPS - 1 - offset
        act_cot = act_cot + conv_weight[offset] * padded_cot[:, shift_start : shift_start + length]
        tap_grads.append(jnp.sum(conv_cot * padded[:, offset : offset + length], axis=(0, 1)))
    return (act_cot, jnp.stack(tap_grads), jnp.sum(conv_cot, axis=(0, 1)))


def contract_last(left, right):
    return lax.dot_general(
        left, right, (((1,), (1,)), ((), ())), preferred_element_type=jnp.float32
    )


def contract_first(left, right):
    return lax.dot_general(
        left, right, (((0,), (0,)), ((), ())), preferred_element_type=jnp.float32
    )


def place(n):
    wide = n // QUADS
    me, tp = lax.axis_index("fs"), lax.axis_index("tp")
    return me // wide, lax.rem(me, wide), tp, lax.rem(tp, 4)


def flip(j, bit):
    return j + bit - 2 * bit * lax.rem(j // bit, 2)


def remote(src, dst, send, recv, fs, tp):
    return pltpu.make_async_remote_copy(
        src_ref=src, dst_ref=dst, send_sem=send, recv_sem=recv,
        device_id=(fs, tp), device_id_type=MESH,
    )


def quarter(width, j):
    return pl.ds(pl.multiple_of((lax.rem(j, 2) * 2 + j // 2) * width, width), width)


def gather_kernel(n, tok, wsrc, tok_all, wall, tz_s, tz_r, tt_s, tt_r, wz_s, wz_r, wx_s, wx_r, own_s):
    wide = n // QUADS
    q, p, tp, j = place(n)
    width = tok.shape[-1] // 4
    base = tp - j
    core, side = base + flip(j, 1), base + flip(j, 2)

    barrier = pltpu.get_barrier_semaphore()
    peers = [(lax.rem(q + d, QUADS) * wide + p, tp) for d in range(1, QUADS)]
    peers += [(q * wide + lax.rem(p + d, wide), tp) for d in range(1, wide)]
    peers += [(q * wide + p, core), (q * wide + p, side)]
    for peer in peers:
        pl.semaphore_signal(barrier, inc=1, device_id=peer, device_id_type=MESH)
    pl.semaphore_wait(barrier, len(peers))

    here = q * wide + p

    def tok_z(src, s, dst_q, way):
        return remote(src, tok_all.at[:, s, :, quarter(width, j)],
                      tz_s.at[s, way], tz_r.at[s], dst_q * wide + p, tp)

    def tok_t(s, place_j, kind, dst):
        cols = quarter(width, place_j)
        return remote(tok_all.at[:, s, :, cols], tok_all.at[:, s, :, cols],
                      tt_s.at[s, kind], tt_r.at[s, place_j], here, dst)

    def w_z(src_q, dst_q):
        return remote(wsrc.at[dst_q], wall.at[src_q * wide + p],
                      wz_s.at[dst_q], wz_r.at[src_q], dst_q * wide + p, tp)

    def w_x(src, s, src_p, dst_p):
        return remote(src, wall.at[s * wide + src_p],
                      wx_s.at[s, dst_p], wx_r.at[s, src_p], q * wide + dst_p, tp)

    started = []

    def go(live, copy):
        @pl.when(live)
        def _():
            copy.start()

        started.append((live, copy))

    always = q >= 0
    own_cols = tok.at[:, :, quarter(width, j)]

    def towards(d, way):
        to = q + d if way == 0 else q - d
        live = to < QUADS if way == 0 else to >= 0
        return lax.rem(to + QUADS, QUADS), live

    def send_weights(d):
        for way in range(2):
            to, live = towards(d, way)
            go(live, w_z(q, to))

    def pass_tokens(d):
        for way in range(2):
            s, there = towards(d, 1 - way)
            onward, more = towards(1, way)
            block = tok_all.at[:, s, :, quarter(width, j)]

            @pl.when(there)
            def _():
                tok_z(own_cols, s, q, 0).wait_recv()

            go(there & more, tok_z(block, s, onward, way))
            go(there, tok_t(s, j, 0, side))
            go(there, tok_t(s, j, 1, core))

    def pass_side(d):
        for way in range(2):
            s, there = towards(d, way)

            @pl.when(there)
            def _():
                tok_t(s, flip(j, 2), 0, side).wait_recv()

            go(there, tok_t(s, flip(j, 2), 2, core))

    def pass_weights(d):
        for way in range(2):
            s, there = towards(d, way)

            @pl.when(there)
            def _():
                w_z(s, q).wait_recv()

            for e in range(1, wide):
                go(there, w_x(wall.at[s * wide + p], s, p, lax.rem(p + e, wide)))

    for way in range(2):
        to, live = towards(1, way)
        go(live, tok_z(own_cols, q, to, way))
    for d in range(1, wide):
        go(always, w_x(wsrc.at[q], q, p, lax.rem(p + d, wide)))
    send_weights(1)
    own_t = pltpu.make_async_copy(tok, tok_all.at[:, q], own_s.at[0])
    own_w = pltpu.make_async_copy(wsrc.at[q], wall.at[q * wide + p], own_s.at[1])
    own_t.start()
    own_w.start()
    pass_tokens(1)
    send_weights(2)
    pass_weights(1)
    pass_tokens(2)
    send_weights(3)
    pass_side(1)
    pass_weights(2)
    pass_tokens(3)
    pass_side(2)
    pass_side(3)
    pass_weights(3)
    for d in range(1, QUADS):
        s = lax.rem(q + d, QUADS)
        tok_t(s, flip(j, 1), 0, core).wait_recv()
        tok_t(s, flip(flip(j, 1), 2), 0, core).wait_recv()
    for s in range(QUADS):
        for e in range(1, wide):
            w_x(wsrc.at[0], s, lax.rem(p + e, wide), p).wait_recv()
    own_t.wait()
    own_w.wait()
    for live, copy in started:
        @pl.when(live)
        def _():
            copy.wait_send()


def scatter_kernel(
    n, gw, gi, small, wout, gout, smalls,
    rx, sw, rc, s1, ry, s2, rg, s3,
    x_s, x_r, z_s, z_r, c_s, c_r, y_s, y_r, g_s, g_r, t_s, t_r, m_s, m_r, own_s,
):
    wide = n // QUADS
    q, p, tp, j = place(n)
    rows = gi.shape[1]
    width = gi.shape[-1] // 4
    base = tp - j
    core, side = base + flip(j, 1), base + flip(j, 2)
    here = q * wide + p
    bit, half = lax.rem(j, 2), j // 2

    barrier = pltpu.get_barrier_semaphore()
    peers = [(lax.rem(here + d, n), tp) for d in range(1, n)]
    peers += [(here, core), (here, side)]
    for peer in peers:
        pl.semaphore_signal(barrier, inc=1, device_id=peer, device_id_type=MESH)
    pl.semaphore_wait(barrier, len(peers))

    started = []

    def go(copy):
        copy.start()
        started.append(copy)

    def at(d):
        return lax.rem(q + d, QUADS)

    def halves(b):
        return pl.ds(pl.multiple_of(b * 2 * width, 2 * width), 2 * width)

    def inner(h):
        return pl.ds(pl.multiple_of(h * width, width), width)

    def c_copy(t):
        return remote(gi.at[t, :, halves(1 - bit)], rc.at[t], c_s.at[t], c_r.at[t], here, core)

    def y_copy(t):
        return remote(s1.at[t, :, inner(1 - half)], ry.at[t], y_s.at[t], y_r.at[t], here, side)

    def g_copy(src_q, t):
        return remote(s2.at[t], rg.at[src_q], g_s.at[t], g_r.at[src_q], t * wide + p, tp)

    def x_copy(src_p, t, dst_p):
        return remote(gw.at[t * wide + dst_p], rx.at[src_p, t], x_s.at[t, dst_p], x_r.at[t, src_p],
                      q * wide + dst_p, tp)

    def z_copy(src_q, t):
        return remote(sw.at[t], wout.at[src_q], z_s.at[t], z_r.at[src_q], t * wide + p, tp)

    def m_copy(src, d):
        return remote(small, smalls.at[src], m_s.at[d], m_r.at[src], d, tp)

    def t_copy(src, place_j, kind, dst):
        return remote(src, gout.at[:, quarter(width, place_j)], t_s.at[kind], t_r.at[place_j], here, dst)

    order = [2, 1, 3, 0]
    for d in order:
        go(c_copy(at(d)))
    for d in order:
        for e in range(1, wide):
            go(x_copy(p, at(d), lax.rem(p + e, wide)))
    for d in range(1, n):
        go(m_copy(here, lax.rem(here + d, n)))
    own_m = pltpu.make_async_copy(small, smalls.at[here], own_s.at[0])
    own_m.start()

    tile = 32 if rows % 32 == 0 else rows

    def rowwise(total, body):
        step = tile if total % tile == 0 else total
        lax.fori_loop(0, total // step, lambda i, c: (body(pl.ds(pl.multiple_of(i * step, step), step)), c)[1], 0)

    def f32(v):
        return v.astype(jnp.float32)

    for d in order:
        t = at(d)
        c_copy(t).wait_recv()

        def add1(r, t=t):
            s1[t, r, :] = (f32(gi[t, r, halves(bit)]) + f32(rc[t, r, :])).astype(s1.dtype)

        rowwise(rows, add1)
        go(y_copy(t))
    for d in order:
        t = at(d)
        for e in range(1, wide):
            x_copy(lax.rem(p + e, wide), t, p).wait_recv()
        for k in range(gw.shape[1]):
            total = f32(gw[t * wide + p, k])
            for e in range(1, wide):
                total = total + f32(rx[lax.rem(p + e, wide), t, k])
            sw[t, k] = total.astype(sw.dtype)
        if d:
            go(z_copy(q, t))
        y_copy(t).wait_recv()

        def add2(r, t=t):
            s2[t, r, :] = (f32(s1[t, r, inner(half)]) + f32(ry[t, r, :])).astype(s2.dtype)

        rowwise(rows, add2)
        if d:
            go(g_copy(q, t))
    own_w = pltpu.make_async_copy(sw.at[q], wout.at[q], own_s.at[1])
    own_w.start()
    for d in range(1, QUADS):
        g_copy(at(d), q).wait_recv()

    def add3(r):
        total = f32(s2[q, r, :])
        for d in range(1, QUADS):
            total = total + f32(rg[at(d), r, :])
        s3[r, :] = total.astype(s3.dtype)

    rowwise(rows, add3)
    go(t_copy(s3, j, 0, side))
    go(t_copy(s3, j, 1, core))
    own_g = pltpu.make_async_copy(s3, gout.at[:, quarter(width, j)], own_s.at[2])
    own_g.start()
    t_copy(s3, flip(j, 2), 0, side).wait_recv()
    go(t_copy(gout.at[:, quarter(width, flip(j, 2))], flip(j, 2), 2, core))
    t_copy(s3, flip(j, 1), 0, core).wait_recv()
    t_copy(s3, flip(flip(j, 1), 2), 0, core).wait_recv()
    for d in range(1, QUADS):
        z_copy(at(d), q).wait_recv()
    for d in range(1, n):
        m_copy(lax.rem(here + d, n), here).wait_recv()
    own_m.wait()
    own_w.wait()
    own_g.wait()
    for copy in started:
        copy.wait_send()


VM = pl.BlockSpec(memory_space=pltpu.VMEM)
DMA = pltpu.SemaphoreType.DMA
BF = jnp.bfloat16


def on_device(
    n, n_tp,
    inputs,
    cotangent,
    up_weight,
    gate_weight,
    down_weight,
    up_scale,
    gate_scale,
    down_scale,
    conv_weight,
    conv_bias,
):
    wide = n // QUADS
    rows, cols = up_weight.shape
    part = cols // QUADS
    tokens, model = inputs.shape
    q = lax.axis_index("fs") // wide

    scaled = (cotangent.astype(jnp.float32) * down_scale).astype(BF)
    tok = jnp.stack([inputs, scaled])
    wsrc = jnp.stack([up_weight.T.astype(BF), gate_weight.T.astype(BF), down_weight.astype(BF)])
    wsrc = wsrc.reshape(3, QUADS, part, rows).transpose(1, 0, 2, 3)

    tok_all, wall = pl.pallas_call(
        functools.partial(gather_kernel, n),
        out_shape=(
            jax.ShapeDtypeStruct((2, QUADS, tokens, model), BF),
            jax.ShapeDtypeStruct((n, 3, part, rows), BF),
        ),
        in_specs=[VM] * 2,
        out_specs=(VM, VM),
        scratch_shapes=[
            DMA((QUADS, 2)), DMA((QUADS,)), DMA((QUADS, 3)), DMA((QUADS, 4)),
            DMA((QUADS,)), DMA((QUADS,)), DMA((QUADS, wide)), DMA((QUADS, wide)), DMA((2,)),
        ],
        compiler_params=pltpu.CompilerParams(
            collective_id=0, has_side_effects=True, vmem_limit_bytes=48 * 2**20
        ),
    )(tok, wsrc)

    full = wall.transpose(1, 2, 0, 3).reshape(3, part, model)
    inp = tok_all[0].reshape(QUADS * tokens, model)
    cot = tok_all[1].reshape(QUADS * tokens, model)

    def mine(v):
        return lax.dynamic_slice_in_dim(v, q * part, part, axis=v.ndim - 1)

    up_s, gate_s, taps, bias = mine(up_scale), mine(gate_scale), mine(conv_weight), mine(conv_bias)
    seq = (QUADS, tokens, part)
    up_act = (contract_last(inp, full[0]) * up_s).reshape(seq)
    gate_act = (contract_last(inp, full[1]) * gate_s).reshape(seq)
    conv_out, padded = causal_conv(up_act, taps, bias)
    gelu_val, gelu_back = jax.vjp(jax.nn.gelu, conv_out)
    hidden = (gelu_val * gate_act).astype(BF).reshape(-1, part)
    hidden_cot = contract_last(cot, full[2]).reshape(seq)
    gate_cot = (hidden_cot * gelu_val * gate_s).astype(BF).reshape(-1, part)
    (conv_cot,) = gelu_back(hidden_cot * gate_act)
    act_cot, tap_part, bias_part = conv_back(conv_cot, padded, taps)
    up_cot = (act_cot * up_s).astype(BF).reshape(-1, part)
    small = jnp.concatenate([tap_part, bias_part[None]], axis=0)
    gi = (jnp.dot(up_cot, full[0], preferred_element_type=jnp.float32)
          + jnp.dot(gate_cot, full[1], preferred_element_type=jnp.float32))
    gi = gi.astype(BF).reshape(QUADS, tokens, model)
    gw = jnp.stack([
        contract_first(up_cot, inp).astype(BF),
        contract_first(gate_cot, inp).astype(BF),
        contract_first(hidden, cot).astype(BF),
    ])
    gw = gw.reshape(3, part, n, rows).transpose(2, 0, 1, 3)

    width = model // 4
    wout, gout, smalls = pl.pallas_call(
        functools.partial(scatter_kernel, n),
        out_shape=(
            jax.ShapeDtypeStruct((QUADS, 3, part, rows), BF),
            jax.ShapeDtypeStruct((tokens, model), BF),
            jax.ShapeDtypeStruct((n,) + small.shape, jnp.float32),
        ),
        in_specs=[VM] * 3,
        out_specs=(VM, VM, VM),
        scratch_shapes=[
            pltpu.VMEM((wide, QUADS, 3, part, rows), BF),
            pltpu.VMEM((QUADS, 3, part, rows), BF),
            pltpu.VMEM((QUADS, tokens, 2 * width), BF),
            pltpu.VMEM((QUADS, tokens, 2 * width), BF),
            pltpu.VMEM((QUADS, tokens, width), BF),
            pltpu.VMEM((QUADS, tokens, width), BF),
            pltpu.VMEM((QUADS, tokens, width), BF),
            pltpu.VMEM((tokens, width), BF),
            DMA((QUADS, wide)), DMA((QUADS, wide)), DMA((QUADS,)), DMA((QUADS,)),
            DMA((QUADS,)), DMA((QUADS,)), DMA((QUADS,)), DMA((QUADS,)),
            DMA((QUADS,)), DMA((QUADS,)), DMA((3,)), DMA((4,)),
            DMA((n,)), DMA((n,)), DMA((3,)),
        ],
        compiler_params=pltpu.CompilerParams(
            collective_id=1, has_side_effects=True, vmem_limit_bytes=56 * 2**20
        ),
    )(gw, gi, small)

    if n_tp > 4:
        groups = [[g * 4 + k for g in range(n_tp // 4)] for k in range(4)]
        gout = lax.psum(gout, "tp", axis_index_groups=groups)
    stats = jnp.sum(smalls.reshape(QUADS, wide, TAPS + 1, part), axis=1)
    stats = stats.transpose(1, 0, 2).reshape(TAPS + 1, cols)
    grads = wout.transpose(1, 0, 2, 3).reshape(3, cols, rows).astype(jnp.float32)
    return (gout, grads[0].T, grads[1].T, grads[2], stats[:TAPS], stats[TAPS])


def solution(mesh):
    in_specs = (
        P("fs", None),
        P("fs", None),
        P("fs", "tp"),
        P("fs", "tp"),
        P("tp", "fs"),
        P("tp"),
        P("tp"),
        P(),
        P(None, "tp"),
        P("tp"),
    )
    out_specs = (P("fs", None), P("fs", "tp"), P("fs", "tp"), P("tp", "fs"), P(None, "tp"), P("tp"))
    return jax.shard_map(
        functools.partial(on_device, mesh.shape["fs"], mesh.shape["tp"]),
        mesh=mesh, in_specs=in_specs, out_specs=out_specs, check_vma=False,
    )
```

profile of v0, /device:TPU:1, one launch (start us, length us, event | category | flops | bytes accessed | tf_op | source)
XLA Modules:
  0.0 188.2 jit_solution(16068744375170594422)
XLA Ops:
  0.6 0.0 copy-start.3
  0.7 0.8 dynamic_slice.15
  1.5 0.8 dynamic_slice.13
  2.2 0.8 dynamic_slice.14
  3.0 0.9 constant_dynamic-slice_fusion
  3.9 1.2 convert_element_type.55
  5.0 0.0 copy-start
  5.1 0.0 copy-start.4
  5.1 1.2 convert_element_type.57
  6.3 0.0 copy-done.3
  6.4 0.0 copy-start.2
  6.4 0.1 maximum_bitcast_fusion.1.wsrc
  6.5 0.0 copy-done
  6.5 0.0 copy-done.4
  6.5 0.2 fusion.2
  6.8 0.9 copy-done.2
  7.6 0.2 pad_maximum_fusion.tok
  7.8 86.2 %shard_map.145 = (bf16[2,4,256,2048]{3,2,1,0:T(8,128)(2,1)}, bf16[8,3,184,256]{3,2,1,0:T(8,128)(2,1)S(1)}) custom-call(bf16[2,256,2048]{2,1,0:T(8,128)(2,1)S(1)} %pad_maximum_fusion.tok, bf16[4,3,184,256]{3,2,1,0:T(8,128)(2,1)S(1)} %maximum_bitcast_fusion.1.wsrc), custom_call_target="tpu_custom_call" | custom-call | tf_op jit(solution)/shard_map/pallas_call | solution.py:362
  94.1 0.1 fusion.23
  94.2 0.1 copy.44
  94.4 0.3 reshape.85
  94.7 0.1 copy.65
  94.8 0.0 slice-start
  94.8 0.1 copy.64
  94.9 0.0 slice-start.1
  94.9 4.3 %fusion.21 = (bf16[1,4,256,2048]{3,2,1,0:T(8,128)(2,1)S(1)}, bf16[1,4,256,2048]{3,2,1,0:T(8,128)(2,1)S(1)}) fusion(bf16[2,4,256,2048]{3,2,1,0:T(8,128)(2,1)} %get-tuple-element.11), kind=kLoop, calls=%fused_computation.50 | loop fusion | bytes 16777216 | tf_op jit(solution)/shard_map/slice | solution.py:381
  99.3 1.5 convolution_multiply_fusion
  100.8 0.1 copy.79
  100.9 1.5 convolution_multiply_fusion.1
  102.4 0.0 slice-done
  102.4 0.0 slice-done.1
  102.5 2.2 %multiply_reduce_fusion.2 = (f32[184]{0:T(256)S(1)}, f32[184]{0:T(256)S(1)}, f32[184]{0:T(256)S(1)}, f32[184]{0:T(256)S(1)}, f32[4,256,184]{1,2,0:T(8,128)S(1)},...) fusion(f32[4,256,184]{1,2,0:T(8,128)S(1)} %bitcast.135, f32[23,4,8,256]{3,2,1,0:T(8,128)S(1)} %bitcast.134, ...), kind=kOutput, calls=%fused_computation.38 | convolution fusion | flops 777968896 | bytes 9476992 | tf_op jit(solution)/shard_map/dot_general | solution.py:37
  104.7 0.6 pad_maximum_fusion.1.small
  105.3 0.7 fusion.16
  106.1 1.0 convolution_convert_fusion
  107.1 0.2 copy.68
  107.3 0.1 copy.56
  107.5 1.0 convolution_convert_fusion.2
  108.5 1.0 convolution_convert_fusion.1
  109.5 0.2 copy.67
  109.7 0.1 copy.55
  109.8 0.2 copy.66
  110.0 0.1 copy.54
  110.2 1.6 maximum_bitcast_fusion.gw
  111.8 1.3 fusion.24
  113.1 3.3 %add_convert_fusion = bf16[1024,2048]{1,0:T(8,128)(2,1)} fusion(f32[1024,2048]{1,0:T(8,128)S(1)} %fusion.24, bf16[1024,184]{0,1:T(8,128)(2,1)S(1)} %bitcast.115, bf16[184,2048]{1,0:T(8,128)(2,1)S(1)} %bitcast.127), kind=kOutput, calls=%fused_computation | convolution fusion | flops 775946240 | bytes 13713408 | tf_op jit(solution)/shard_map/dot_general | solution.py:400
  116.4 65.4 %shard_map.146 = (bf16[4,3,184,256]{3,2,1,0:T(8,128)(2,1)}, bf16[256,2048]{1,0:T(8,128)(2,1)}, f32[8,4,184]{2,1,0:T(4,128)}) custom-call(bf16[8,3,184,256]{3,2,1,0:T(8,128)(2,1)} %maximum_bitcast_fusion.gw, bf16[4,256,2048]{2,1,0:T(8,128)(2,1)} %bitcast.109, f32[4,184]{1,0:T(4,128)} %pad_maximum_fusion.1.small), custom_call_target="tpu_custom_call" | custom-call | tf_op jit(solution)/shard_map/pallas_call | solution.py:410
  181.8 0.8 bitcast_reduce_fusion
  182.6 0.7 squeeze.29
  183.3 0.7 slice.87
  184.0 1.4 convert_bitcast_fusion
  185.4 0.0 copy-start.1
  185.4 1.4 fusion.22
  186.8 0.4 copy-done.1
  187.2 1.0 copy.81
  (7 shorter events, 0.2 us)
Async XLA Ops:
  0.6 5.7 %copy-start.3 = (f32[736,256]{1,0:T(8,128)S(1)}, f32[736,256]{1,0:T(8,128)}, u32[]{:S(2)}) copy-start(f32[736,256]{1,0:T(8,128)} %param.14) | copy-start | bytes 2260996
  5.0 1.5 copy-start
  5.1 1.5 copy-start.4
  6.4 1.3 copy-start.2
  94.8 7.6 %slice-start = ((s8[8388608]{0:T(1024)(128)(4,1)}), s8[4194304]{0:T(1024)(128)(4,1)S(1)}, s32[]{:S(2)}) async-start(s8[8388608]{0:T(1024)(128)(4,1)} %bitcast.110), calls=%async_computation | async-start | bytes 8388608
  94.9 7.5 %slice-start.1 = ((s8[8388608]{0:T(1024)(128)(4,1)}), s8[4194304]{0:T(1024)(128)(4,1)S(1)}, s32[]{:S(2)}) async-start(s8[8388608]{0:T(1024)(128)(4,1)} %bitcast.110), calls=%async_computation.1 | async-start | bytes 8388608
  185.4 1.8 copy-start.1
where the time goes:
time: 190 us; the launch traced here: 188 us
  Pallas kernels  152 us (80%)
  local copies, waits for them, and re-layouts  14.6 us (8%)
  matrix products  12.9 us (7%)
  other arithmetic  8.05 us (4%)
    pallas_call x1, Pallas kernels, on_device(): pl.pallas_call(functools.partial(gather_kernel, n), out_shape=(jax.ShapeD...  86.2 us
    pallas_call x1, Pallas kernels, on_device(): pl.pallas_call(functools.partial(scatter_kernel, n), out_shape=(jax.Shape...  65.4 us
    dot_general x3, matrix products, contract_last(): lax.dot_general(left, right, (((1,), (1,)), ((), ())), preferred_element_...  5.34 us
    slice x1, local copies, waits for them, and re-layouts, on_device(): cot = tok_all[1].reshape(QUADS * tokens, model)  4.32 us

commit v1 on v0

--- a/solution.py
+++ b/solution.py
@@ -335,7 +335,7 @@
 BF = jnp.bfloat16
 
 
-def on_device(
+def general(
     n, n_tp,
     inputs,
     cotangent,
@@ -444,6 +444,469 @@
     return (gout, grads[0].T, grads[1].T, grads[2], stats[:TAPS], stats[TAPS])
 
 
+LANES = 128
+CHUNKS = 2
+BLOCK = 512
+ROOT_2_PI = 0.7978845608028654
+CUBIC = 0.044715
+
+
+def follow(q):
+    near = flip(q, 1)
+    far = jnp.where(q < 2, 2, 1)
+    last = jnp.where(q < 2, 3, 0)
+    return [q, near, far, last]
+
+
+def fused_kernel(
+    n, inp, cot, dscale, wsrc, par, wout, gout, smalls,
+    tok, wall, ct, gi, acc, gw, rx, sw, rc, s1, ry, s2, rz, s3, sm, small,
+    tz_s, tz_r, tt_s, tt_r, wz_s, wz_r, wx_s, wx_r,
+    c_s, c_r, y_s, y_r, g_s, g_r, t_s, t_r, x_s, x_r, z_s, z_r, m_s, m_r, own_s,
+):
+    wide = n // QUADS
+    q, p, tp, j = place(n)
+    tokens, model = inp.shape
+    rows = wsrc.shape[-1]
+    deep = ct.shape[1]
+    width = model // 4
+    base = tp - j
+    core, side = base + flip(j, 1), base + flip(j, 2)
+    here = q * wide + p
+    bit, half = lax.rem(j, 2), j // 2
+    last = QUADS - 1
+    seqs = follow(q)
+    always = q >= 0
+    pieces = 2 * CHUNKS
+    span = tokens // CHUNKS
+
+    started = []
+
+    def go(live, copy):
+        if live is always:
+            copy.start()
+        else:
+            @pl.when(live)
+            def _():
+                copy.start()
+
+        started.append((live, copy))
+
+    def f32(v):
+        return v.astype(jnp.float32)
+
+    def halves(b):
+        return pl.ds(pl.multiple_of(b * 2 * width, 2 * width), 2 * width)
+
+    def inner(h):
+        return pl.ds(pl.multiple_of(h * width, width), width)
+
+    def owned(fs):
+        return pl.ds(pl.multiple_of(fs * rows, rows), rows)
+
+    def piece(s, k, place_j):
+        return tok.at[k // CHUNKS, s, pl.ds(k % CHUNKS * span, span), quarter(width, place_j)]
+
+    def tok_z(s, k, way, dst_q):
+        return remote(piece(s, k, j), piece(s, k, j), tz_s.at[s, way, k], tz_r.at[s, k], dst_q * wide + p, tp)
+
+    def tok_t(s, k, place_j, kind, dst):
+        ref = piece(s, k, place_j)
+        return remote(ref, ref, tt_s.at[s, kind, k], tt_r.at[s, place_j, k], here, dst)
+
+    def w_z(src_q, dst_q):
+        return remote(wsrc.at[dst_q], wall.at[:, :, owned(src_q * wide + p)],
+                      wz_s.at[dst_q], wz_r.at[src_q], dst_q * wide + p, tp)
+
+    def w_x(src, s, src_p, dst_p):
+        return remote(src, wall.at[:, :, owned(s * wide + src_p)],
+                      wx_s.at[s, dst_p], wx_r.at[s, src_p], q * wide + dst_p, tp)
+
+    def c_copy(t):
+        return remote(gi.at[t, :, halves(1 - bit)], rc.at[t], c_s.at[t], c_r.at[t], here, core)
+
+    def y_copy(t):
+        return remote(s1.at[t, :, inner(1 - half)], ry.at[t], y_s.at[t], y_r.at[t], here, side)
+
+    def g_copy(t, slot, dst_q):
+        return remote(s2.at[t], rz.at[slot], g_s.at[t], g_r.at[slot], dst_q * wide + p, tp)
+
+    def x_copy(src_p, t, dst_p):
+        return remote(gw.at[:, :, owned(t * wide + dst_p)], rx.at[src_p, t],
+                      x_s.at[t, dst_p], x_r.at[t, src_p], q * wide + dst_p, tp)
+
+    def z_copy(src_q, t):
+        return remote(sw.at[t], wout.at[src_q], z_s.at[t], z_r.at[src_q], t * wide + p, tp)
+
+    def m_copy(src, d):
+        return remote(small, smalls.at[src], m_s.at[d], m_r.at[src], d, tp)
+
+    def t_copy(src, place_j, kind, dst):
+        return remote(src, gout.at[:, quarter(width, place_j)], t_s.at[kind], t_r.at[place_j], here, dst)
+
+    tile = 32 if tokens % 32 == 0 else tokens
+
+    def rowwise(total, body):
+        lax.fori_loop(0, total // tile, lambda i, c: (body(pl.ds(pl.multiple_of(i * tile, tile), tile)), c)[1], 0)
+
+    barrier = pltpu.get_barrier_semaphore()
+    peers = [(lax.rem(here + d, n), tp) for d in range(1, n)]
+    peers += [(here, core), (here, side)]
+    for peer in peers:
+        pl.semaphore_signal(barrier, inc=1, device_id=peer, device_id_type=MESH)
+
+    def prepare(r):
+        tok[0, q, r, :] = inp[r, :]
+        tok[1, q, r, :] = (f32(cot[r, :]) * dscale[...]).astype(tok.dtype)
+
+    rowwise(tokens, prepare)
+    sm[...] = jnp.zeros_like(sm)
+    pl.semaphore_wait(barrier, len(peers))
+
+    for e in range(1, wide):
+        go(always, w_x(wsrc.at[q], q, p, lax.rem(p + e, wide)))
+    for d in range(1, QUADS):
+        for way in range(2):
+            to = q + d if way == 0 else q - d
+            live = to < QUADS if way == 0 else to >= 0
+            go(live, w_z(q, lax.rem(to + QUADS, QUADS)))
+    for k in range(pieces):
+        go(q < last, tok_z(q, k, 0, lax.rem(q + 1, QUADS)))
+        go(q > 0, tok_z(q, k, 1, lax.rem(q + last, QUADS)))
+    own_w = pltpu.make_async_copy(wsrc.at[q], wall.at[:, :, owned(here)], own_s.at[0])
+    own_w.start()
+
+    def beyond(s):
+        more = ((s < q) & (q < last)) | ((s > q) & (q > 0))
+        return more, lax.rem(jnp.where(s < q, q + 1, q + last), QUADS)
+
+    def relay(i, k):
+        s = seqs[i]
+        more, onward = beyond(s)
+        tok_z(s, k, 0, q).wait_recv()
+        go(more, tok_z(s, k, 0, onward))
+        go(always, tok_t(s, k, j, 0, side))
+        go(always, tok_t(s, k, j, 1, core))
+
+    def relay_side(i, k):
+        s = seqs[i]
+        tok_t(s, k, flip(j, 2), 0, side).wait_recv()
+        go(always, tok_t(s, k, flip(j, 2), 2, core))
+
+    def arrive(i):
+        s = seqs[i]
+        for k in range(pieces):
+            tok_t(s, k, flip(j, 1), 0, core).wait_recv()
+            tok_t(s, k, flip(flip(j, 1), 2), 0, core).wait_recv()
+
+    def forward(s):
+        up_s, gate_s = par[q, :, 0:1], par[q, :, 1:2]
+        tap = [par[q, :, 2 + k : 3 + k] for k in range(TAPS)]
+        bias = par[q, :, 5:6]
+        both = contract_last(wall[0:2].reshape(2 * deep, model), tok[0, s])
+        up, gate = both[:deep] * up_s, both[deep:] * gate_s
+        lane = lax.broadcasted_iota(jnp.int32, up.shape, 1)
+        zero = jnp.zeros_like(up)
+        late = [jnp.where(lane < TAPS - 1 - k, zero, pltpu.roll(up, TAPS - 1 - k, 1)) for k in range(TAPS - 1)] + [up]
+        v = bias + tap[0] * late[0] + tap[1] * late[1] + tap[2] * late[2]
+        square = v * v
+        t = jnp.tanh(ROOT_2_PI * (v + CUBIC * (square * v)))
+        rise = 0.5 * (1.0 + t)
+        value = v * rise
+        slope = rise + 0.5 * v * (1.0 - t * t) * (ROOT_2_PI * (1.0 + 3.0 * CUBIC * square))
+        ct[2] = (value * gate).astype(ct.dtype)
+        back = contract_last(wall[2], tok[1, s])
+        ct[1] = (back * value * gate_s).astype(ct.dtype)
+        conv_cot = back * gate * slope
+        act_cot = tap[2] * conv_cot
+        for k in range(TAPS - 1):
+            early = pltpu.roll(conv_cot, tokens - (TAPS - 1 - k), 1)
+            act_cot = act_cot + tap[k] * jnp.where(lane >= tokens - (TAPS - 1 - k), zero, early)
+        ct[0] = (act_cot * up_s).astype(ct.dtype)
+        sums = [jnp.sum(conv_cot * late[k], axis=1, keepdims=True) for k in range(TAPS)]
+        sums.append(jnp.sum(conv_cot, axis=1, keepdims=True))
+        for k, total in enumerate(sums):
+            sm[0:deep, k : k + 1] = sm[0:deep, k : k + 1] + total
+
+    def half_input(s, b):
+        def block(i, carry):
+            at = pl.ds(pl.multiple_of(b * 2 * width + i * BLOCK, BLOCK), BLOCK)
+            total = contract_first(ct[0], wall[0, :, at]) + contract_first(ct[1], wall[1, :, at])
+            gi[s, :, at] = total.astype(gi.dtype)
+            return carry
+
+        lax.fori_loop(0, 2 * width // BLOCK, block, 0)
+
+    def input_grad(s):
+        half_input(s, 1 - bit)
+        go(always, c_copy(s))
+        half_input(s, bit)
+
+    def product(s, at):
+        first = jnp.dot(ct[0:2].reshape(2 * deep, tokens), tok[0, s, :, at], preferred_element_type=jnp.float32)
+        second = jnp.dot(ct[2], tok[1, s, :, at], preferred_element_type=jnp.float32)
+        return first.reshape(2, deep, first.shape[-1]), second
+
+    def weight_grad(s, fresh):
+        def block(i, carry):
+            at = pl.ds(pl.multiple_of(i * BLOCK, BLOCK), BLOCK)
+            first, second = product(s, at)
+            if fresh:
+                acc[0:2, :, at] = first
+                acc[2, :, at] = second
+            else:
+                acc[0:2, :, at] = acc[0:2, :, at] + first
+                acc[2, :, at] = acc[2, :, at] + second
+            return carry
+
+        lax.fori_loop(0, model // BLOCK, block, 0)
+
+    def close(s, fs):
+        at = owned(fs)
+        first, second = product(s, at)
+        gw[0:2, :, at] = (acc[0:2, :, at] + first).astype(gw.dtype)
+        gw[2, :, at] = (acc[2, :, at] + second).astype(gw.dtype)
+
+    def core_sum(t):
+        c_copy(t).wait_recv()
+
+        def add(r):
+            s1[t, r, :] = (f32(gi[t, r, halves(bit)]) + f32(rc[t, r, :])).astype(s1.dtype)
+
+        rowwise(tokens, add)
+        go(always, y_copy(t))
+
+    def side_sum(t):
+        y_copy(t).wait_recv()
+
+        def add(r):
+            s2[t, r, :] = (f32(s1[t, r, inner(half)]) + f32(ry[t, r, :])).astype(s2.dtype)
+
+        rowwise(tokens, add)
+
+    def chain(i):
+        s = seqs[i]
+        more, _ = beyond(s)
+        onward = lax.rem(jnp.where(s < q, q + last, q + 1), QUADS)
+        slot = jnp.where((onward == s) & (s < q), QUADS, s)
+
+        @pl.when(more)
+        def _():
+            g_copy(s, s, q).wait_recv()
+
+            def add(r):
+                s2[s, r, :] = (f32(s2[s, r, :]) + f32(rz[s, r, :])).astype(s2.dtype)
+
+            rowwise(tokens, add)
+
+        go(always, g_copy(s, slot, onward))
+
+    def send_grads(t):
+        for e in range(1, wide):
+            dst = lax.rem(p + e, wide)
+            close(seqs[-1], t * wide + dst)
+            go(always, x_copy(p, t, dst))
+        close(seqs[-1], t * wide + p)
+
+    def pass_grads(t, live):
+        for e in range(1, wide):
+            x_copy(lax.rem(p + e, wide), t, p).wait_recv()
+
+        def add(i, carry):
+            k, r = i // (deep // 8), pl.ds(pl.multiple_of(lax.rem(i, deep // 8) * 8, 8), 8)
+            total = f32(gw[k, r, owned(t * wide + p)])
+            for e in range(1, wide):
+                total = total + f32(rx[lax.rem(p + e, wide), t, k, r, :])
+            sw[t, k, r, :] = total.astype(sw.dtype)
+            return carry
+
+        for k in range(3):
+            total = f32(gw[k, :, owned(t * wide + p)])
+            for e in range(1, wide):
+                total = total + f32(rx[lax.rem(p + e, wide), t, k])
+            sw[t, k] = total.astype(sw.dtype)
+        if live:
+            go(always, z_copy(q, t))
+
+    for i in range(1, QUADS):
+        s = seqs[i]
+        w_z(s, q).wait_recv()
+        for e in range(1, wide):
+            go(always, w_x(wall.at[:, :, owned(s * wide + p)], s, p, lax.rem(p + e, wide)))
+    own_w.wait()
+    for i in range(QUADS):
+        for e in range(1, wide):
+            w_x(wsrc.at[0], seqs[i], lax.rem(p + e, wide), p).wait_recv()
+
+    for i in range(QUADS - 1):
+        s = seqs[i]
+        for k in range(CHUNKS):
+            relay(i + 1, k)
+        if i:
+            arrive(i)
+        forward(s)
+        for k in range(CHUNKS, pieces):
+            relay(i + 1, k)
+        input_grad(s)
+        for k in range(pieces):
+            relay_side(i + 1, k)
+        weight_grad(s, i == 0)
+        if i:
+            side_sum(seqs[i - 1])
+        core_sum(s)
+    s = seqs[-1]
+    arrive(QUADS - 1)
+    forward(s)
+    input_grad(s)
+    order = [seqs[3], seqs[2], seqs[1], seqs[0]]
+    send_grads(order[0])
+    core_sum(s)
+    send_grads(order[1])
+    side_sum(seqs[2])
+    chain(2)
+    send_grads(order[2])
+    side_sum(seqs[3])
+    chain(3)
+    send_grads(order[3])
+    flat = sm[...].T
+    small[...] = flat[0 : small.shape[0], :]
+    for d in range(1, n):
+        go(always, m_copy(here, lax.rem(here + d, n)))
+    own_m = pltpu.make_async_copy(small, smalls.at[here], own_s.at[1])
+    own_m.start()
+    pass_grads(order[0], True)
+    pass_grads(order[1], True)
+    chain(1)
+    pass_grads(order[2], True)
+    pass_grads(order[3], False)
+    own_g = pltpu.make_async_copy(sw.at[q], wout.at[q], own_s.at[2])
+    own_g.start()
+
+    def seed(r):
+        s3[r, :] = f32(s2[q, r, :])
+
+    rowwise(tokens, seed)
+    for live, slot in ((q > 0, q), (q < last, QUADS)):
+        @pl.when(live)
+        def _(slot=slot):
+            g_copy(q, slot, q).wait_recv()
+
+            def add(r):
+                s3[r, :] = s3[r, :] + f32(rz[slot, r, :])
+
+            rowwise(tokens, add)
+
+    mine = quarter(width, j)
+
+    def finish(r):
+        gout[r, mine] = s3[r, :].astype(gout.dtype)
+
+    rowwise(tokens, finish)
+    go(always, t_copy(gout.at[:, mine], j, 0, side))
+    go(always, t_copy(gout.at[:, mine], j, 1, core))
+    t_copy(gout.at[:, mine], flip(j, 2), 0, side).wait_recv()
+    go(always, t_copy(gout.at[:, quarter(width, flip(j, 2))], flip(j, 2), 2, core))
+    t_copy(gout.at[:, mine], flip(j, 1), 0, core).wait_recv()
+    t_copy(gout.at[:, mine], flip(flip(j, 1), 2), 0, core).wait_recv()
+    for i in range(1, QUADS):
+        z_copy(seqs[i], q).wait_recv()
+    for d in range(1, n):
+        m_copy(lax.rem(here + d, n), here).wait_recv()
+    own_m.wait()
+    own_g.wait()
+    for live, copy in started:
+        if live is always:
+            copy.wait_send()
+        else:
+            @pl.when(live)
+            def _():
+                copy.wait_send()
+
+
+def fused(
+    n, n_tp,
+    inputs,
+    cotangent,
+    up_weight,
+    gate_weight,
+    down_weight,
+    up_scale,
+    gate_scale,
+    down_scale,
+    conv_weight,
+    conv_bias,
+):
+    wide = n // QUADS
+    rows, cols = up_weight.shape
+    part = cols // QUADS
+    deep = -(-part // 16) * 16
+    tall = -(-deep // LANES) * LANES
+    tokens, model = inputs.shape
+    width = model // 4
+
+    wsrc = jnp.stack([up_weight.T.astype(BF), gate_weight.T.astype(BF), down_weight.astype(BF)])
+    wsrc = wsrc.reshape(3, QUADS, part, rows).transpose(1, 0, 2, 3)
+    wsrc = jnp.pad(wsrc, ((0, 0), (0, 0), (0, deep - part), (0, 0)))
+    par = jnp.concatenate([up_scale[None], gate_scale[None], conv_weight, conv_bias[None]], axis=0)
+    par = par.reshape(TAPS + 3, QUADS, part).transpose(1, 2, 0)
+    par = jnp.pad(par, ((0, 0), (0, deep - part), (0, LANES - TAPS - 3)))
+
+    pieces = 2 * CHUNKS
+    wout, gout, smalls = pl.pallas_call(
+        functools.partial(fused_kernel, n),
+        out_shape=(
+            jax.ShapeDtypeStruct((QUADS, 3, deep, rows), BF),
+            jax.ShapeDtypeStruct((tokens, model), BF),
+            jax.ShapeDtypeStruct((n, 8, tall), jnp.float32),
+        ),
+        in_specs=[VM] * 5,
+        out_specs=(VM, VM, VM),
+        scratch_shapes=[
+            pltpu.VMEM((2, QUADS, tokens, model), BF),
+            pltpu.VMEM((3, deep, model), BF),
+            pltpu.VMEM((3, deep, tokens), BF),
+            pltpu.VMEM((QUADS, tokens, model), BF),
+            pltpu.VMEM((3, deep, model), jnp.float32),
+            pltpu.VMEM((3, deep, model), BF),
+            pltpu.VMEM((wide, QUADS, 3, deep, rows), BF),
+            pltpu.VMEM((QUADS, 3, deep, rows), BF),
+            pltpu.VMEM((QUADS, tokens, 2 * width), BF),
+            pltpu.VMEM((QUADS, tokens, 2 * width), BF),
+            pltpu.VMEM((QUADS, tokens, width), BF),
+            pltpu.VMEM((QUADS, tokens, width), BF),
+            pltpu.VMEM((QUADS + 1, tokens, width), BF),
+            pltpu.VMEM((tokens, width), jnp.float32),
+            pltpu.VMEM((tall, LANES), jnp.float32),
+            pltpu.VMEM((8, tall), jnp.float32),
+            DMA((QUADS, 2, pieces)), DMA((QUADS, pieces)), DMA((QUADS, 3, pieces)), DMA((QUADS, 4, pieces)),
+            DMA((QUADS,)), DMA((QUADS,)), DMA((QUADS, wide)), DMA((QUADS, wide)),
+            DMA((QUADS,)), DMA((QUADS,)), DMA((QUADS,)), DMA((QUADS,)),
+            DMA((QUADS,)), DMA((QUADS + 1,)), DMA((3,)), DMA((4,)),
+            DMA((QUADS, wide)), DMA((QUADS, wide)), DMA((QUADS,)), DMA((QUADS,)),
+            DMA((n,)), DMA((n,)), DMA((3,)),
+        ],
+        compiler_params=pltpu.CompilerParams(
+            collective_id=2, has_side_effects=True, vmem_limit_bytes=60 * 2**20
+        ),
+    )(inputs, cotangent, down_scale[None], wsrc, par)
+
+    if n_tp > 4:
+        groups = [[g * 4 + k for g in range(n_tp // 4)] for k in range(4)]
+        gout = lax.psum(gout, "tp", axis_index_groups=groups)
+    stats = jnp.sum(smalls.reshape(QUADS, wide, 8, tall)[:, :, : TAPS + 1, :part], axis=1)
+    stats = stats.transpose(1, 0, 2).reshape(TAPS + 1, cols)
+    grads = wout[:, :, :part].transpose(1, 0, 2, 3).reshape(3, cols, rows).astype(jnp.float32)
+    return (gout, grads[0].T, grads[1].T, grads[2], stats[:TAPS], stats[TAPS])
+
+
+def on_device(n, n_tp, inputs, cotangent, up_weight, *rest):
+    rows, cols = up_weight.shape
+    part, (tokens, model) = cols // QUADS, inputs.shape
+    even = rows % LANES == 0 and part % 8 == 0 and tokens % LANES == 0 and model % (4 * BLOCK) == 0
+    plan = fused if even and n == 2 * QUADS else general
+    return plan(n, n_tp, inputs, cotangent, up_weight, *rest)
+
+
 def solution(mesh):
     in_specs = (
         P("fs", None),

time: 190 us -> 174 us (0.916)
  matrix products: 12.9 us -> 0 us
  Pallas kernels: 152 us -> 160 us
  other arithmetic: 8.05 us -> 2.53 us
  local copies, waits for them, and re-layouts: 14.6 us -> 10.5 us
    dot_general x8 -> x0, matrix products: 12.9 us -> none  [the longest x3 5.34 us: contract_last(): lax.dot_general(left, right, (((1,), (1,)), ((), ())), preferred_element_...]
    pallas_call x2 -> x1, Pallas kernels: 152 us -> 160 us  [fused(): pl.pallas_call(functools.partial(fused_kernel, n), out_shape=(jax.ShapeDt...]
    slice x8 -> x4, local copies, waits for them, and re-layouts: 7.63 us -> 2.13 us  [fused(): return (gout, grads[0].T, grads[1].T, grads[2], stats[:TAPS], stats[TAPS])]
    concatenate x0 -> x5, local copies, waits for them, and re-layouts: none -> 3.35 us  [fused(): jnp.concatenate([up_scale[None], gate_scale[None], conv_weight, conv_bias...]
    dynamic_slice x3 -> x0, local copies, waits for them, and re-layouts: 2.35 us -> none  [mine(): return lax.dynamic_slice_in_dim(v, q * part, part, axis=v.ndim - 1)]
    convert_element_type x4, other arithmetic: 3.87 us -> 1.54 us  [the longest x1 1.42 us: fused(): wout[:, :, :part].transpose(1, 0, 2, 3).reshape(3, cols, rows)]
where the time goes in v1:
time: 174 us
  Pallas kernels  160 us (92%)
  local copies, waits for them, and re-layouts  10.5 us (6%)
  other arithmetic  2.53 us (1%)
    pallas_call x1, Pallas kernels, fused(): pl.pallas_call(functools.partial(fused_kernel, n), out_shape=(jax.ShapeDt...  160 us

profile of v1, /device:TPU:1, one launch (start us, length us, event | category | flops | bytes accessed | tf_op | source)
XLA Modules:
  0.0 173.8 jit_solution(137275823406927633)
XLA Ops:
  0.6 0.0 copy-start.1
  0.6 0.8 concatenate.13
  1.5 0.8 concatenate.14
  2.2 0.8 concatenate.16
  3.0 0.8 concatenate.15
  3.8 0.0 copy-start.2
  3.8 0.2 copy.22
  4.0 0.8 pad.9.par
  4.8 0.0 copy-done.1
  4.8 0.0 copy-start.3
  4.8 0.1 copy-done.2
  5.0 1.0 copy-done.3
  6.0 0.1 maximum_bitcast_fusion
  6.1 1.1 pad.8.wsrc
  7.3 160.1 %shard_map.145 = (bf16[4,3,192,256]{3,2,1,0:T(8,128)(2,1)}, bf16[256,2048]{1,0:T(8,128)(2,1)}, f32[8,8,256]{2,1,0:T(8,128)}) custom-call(bf16[256,2048]{1,0:T(8,128)(2,1)} %inp.1, bf16[256,2048]{1,0:T(8,128)(2,1)} %cot.1, f32[1,2048]{1,0:T(1,128)} %bitcast.33, bf16[4,3,192,256]{3,2,1,0:T(8,128)(2,1)} %pad.8.wsrc, f32[4,192,128]{2,1,0:T(8,128)} %pad.9.par), custom_call_target="tpu_custom_call" | custom-call | tf_op jit(solution)/shard_map/pallas_call | solution.py:855
  167.4 0.9 slice_reduce_fusion
  168.2 0.7 squeeze.15
  168.9 0.7 slice.34
  169.6 1.4 convert_bitcast_fusion
  171.0 0.0 copy-start
  171.1 1.4 fusion
  172.5 0.4 copy-done
  172.9 1.0 copy.25
  (6 shorter events, 0.2 us)
Async XLA Ops:
  0.6 4.2 %copy-start.1 = (f32[256,736]{0,1:T(8,128)S(1)}, f32[256,736]{0,1:T(8,128)}, u32[]{:S(2)}) copy-start(f32[256,736]{0,1:T(8,128)} %param.12) | copy-start | bytes 2260996
  3.8 1.1 copy-start.2
  4.8 1.2 copy-start.3
  171.0 1.8 %copy-start = (bf16[256,2048]{1,0:T(8,128)(2,1)S(1)}, bf16[256,2048]{1,0:T(8,128)(2,1)}, u32[]{:S(2)}) copy-start(bf16[256,2048]{1,0:T(8,128)(2,1)} %get-tuple-element.21) | copy-start | bytes 3145732
